TPU v7x, 1024 devices: a whole 4x4x32 slice. The times are simulated.
1024 devices in a mesh: ep: 64 (over z, core), tp: 16 (over y, x).
Axes of the slice: x: 4, y: 4, z: 32, core: 2. Of those that a mesh axis runs over, the one named last changes fastest.
Arguments:
- resid_in: bfloat16 [2048, 2048], P('ep'), may hold values from -10 to 10
- state_in: float32 [2048, 1024, 128], P('ep', 'tp'), may hold values from -6 to 6
- mix_gain: bfloat16 [2048], replicated, may hold values from 0.099609375 to 1.8984375
- query_weight: bfloat16 [2048, 512], replicated, may hold values from -0.125 to 0.125
- key_weight: bfloat16 [2048, 512], replicated, may hold values from -0.125 to 0.125
- decay_weight: bfloat16 [2048, 512], replicated, may hold values from -0.375 to 0.375
- value_weight: bfloat16 [2048, 1024], P(None, 'tp'), may hold values from -0.125 to 0.125
- decay_bias: float32 [512], replicated, may hold values from -12 to 4
- proj_weight: bfloat16 [1024, 2048], P('tp'), may hold values from -0.25 to 0.25
- ffn_gain: bfloat16 [2048], P('tp'), may hold values from 0.099609375 to 1.8984375
- expert_gate: bfloat16 [64, 2048, 256], P('ep', 'tp'), may hold values from -0.125 to 0.125
- expert_up: bfloat16 [64, 2048, 256], P('ep', 'tp'), may hold values from -0.125 to 0.125
- expert_down: bfloat16 [64, 256, 2048], P('ep', None, 'tp'), may hold values from -0.375 to 0.375
- route_group: int32 [2048], replicated, may hold values from 0 to 15, as said below
- route_pick: int32 [2048, 2], replicated, may hold values from 0 to 3, as said below
- route_weight: float32 [2048, 2], replicated, may hold values from 0.2 to 1
Outputs:
- resid_out: bfloat16 [2048, 2048], P('ep', 'tp')
- state_out: float32 [2048, 1024, 128], P('ep', 'tp')
Inputs may be any that keep to these rules, and one draw needn't show every extreme that they name: `route_group`: group g holds experts 4 * g to 4 * g + 3. Among the 32 tokens of one aligned block, no expert is named by more than 2 pairs (token, k), and in every draw some expert is named by exactly 2 pairs in every block. `route_pick`: the 2 entries of a token differ.
All inputs are finite; a program needn't handle non-finite values.
Results may differ from a plain program's by a relative error of at most 0.015.
Values may be sent and summed in bfloat16 or wider, within the bound.
A program may use at most 64 MiB of HBM per device.

v0:
```python
import functools

import jax
import jax.numpy as jnp
from jax import lax
from jax.sharding import Mesh
from jax.sharding import PartitionSpec as P

DV = 256
EPG = 4
TOPK = 2
TP = ("tp_0", "tp_1")
EP = ("ep_0", "ep_1")


epsilon = 1e-06
gate_tau = 16.0


def cut_along(shard, dim, devices):
    dims = shard.shape
    pieces = shard.reshape(*dims[:dim], devices, dims[dim] // devices, *dims[dim + 1 :])
    return jnp.moveaxis(pieces, dim, 0)


def summed_on_arrival(shard, axis, dim):
    pieces = cut_along(shard, dim, lax.axis_size(axis))
    arrived = lax.all_to_all(pieces, axis, split_axis=0, concat_axis=0, tiled=True)
    return arrived.astype(jnp.float32).sum(axis=0)


def one_axis_at_a_time(shard, axes):
    return functools.reduce(lax.psum, axes, shard)


def joined_along(pieces, dim):
    pieces = jnp.moveaxis(pieces, 0, dim)
    dims = pieces.shape
    return pieces.reshape(*dims[:dim], dims[dim] * dims[dim + 1], *dims[dim + 2 :])


def copy_for_each(shard, axis):
    devices = lax.axis_size(axis)
    return lax.all_to_all(
        jnp.broadcast_to(shard[None], (devices, *shard.shape)), axis, 0, 0, tiled=True
    )


def collect(shard, axis, dim):
    return joined_along(copy_for_each(shard, axis), dim)


def moved_by_axis(pieces, axes, order):
    dims = [lax.axis_size(a) for a in axes]
    pieces = pieces.reshape(*dims, *pieces.shape[1:])
    for k in order:
        pieces = lax.all_to_all(pieces, axes[k], split_axis=k, concat_axis=k, tiled=True)
    return pieces.reshape(-1, *pieces.shape[len(axes) :])


def core_and_chips(shard, groups, order, split_dim, concat_dim):
    devices = lax.axis_size(groups[0]) * lax.axis_size(groups[1])
    pieces = cut_along(shard, split_dim, devices)
    return joined_along(moved_by_axis(pieces, groups, order), concat_dim)


def inverse_rms(values):
    return lax.rsqrt(jnp.mean(values * values, axis=-1, keepdims=True) + epsilon)


def pair_slots(expert_ids, expert_count):
    onehot = (expert_ids[..., None] == jnp.arange(expert_count, dtype=jnp.int32)).astype(jnp.int32)
    earlier = jnp.cumsum(onehot, axis=-2) - onehot
    return jnp.sum(earlier * onehot, axis=-1)


def on_device(
    resid_in,
    state_in,
    mix_gain,
    query_weight,
    key_weight,
    decay_weight,
    value_weight,
    decay_bias,
    proj_weight,
    ffn_gain,
    expert_gate,
    expert_up,
    expert_down,
    route_group,
    route_pick,
    route_weight,
):
    seq_count = resid_in.shape[0]
    model_width = resid_in.shape[1]
    tp_count = lax.axis_size(TP)
    tp_index = lax.axis_index(TP)
    ep_count = lax.axis_size(EP)
    ep_index = lax.axis_index(EP)
    value_cols = state_in.shape[1]
    key_dim = state_in.shape[2]
    part_width = model_width // tp_count
    row_values = resid_in.astype(jnp.float32)
    normed_in = (row_values * inverse_rms(row_values) * mix_gain.astype(jnp.float32)).astype(
        jnp.bfloat16
    )
    head_start = tp_index * value_cols // DV * key_dim
    query_head = lax.dynamic_slice_in_dim(query_weight, head_start, key_dim, 1)
    key_head = lax.dynamic_slice_in_dim(key_weight, head_start, key_dim, 1)
    decay_head = lax.dynamic_slice_in_dim(decay_weight, head_start, key_dim, 1)
    queries = (
        jnp.dot(normed_in, query_head, preferred_element_type=jnp.float32) * key_dim ** (-0.5)
    ).astype(jnp.bfloat16)
    key_rows = jnp.dot(normed_in, key_head, preferred_element_type=jnp.float32).astype(jnp.bfloat16)
    decay_rows = jnp.dot(normed_in, decay_head, preferred_element_type=jnp.float32).astype(
        jnp.bfloat16
    )
    value_rows = jnp.dot(normed_in, value_weight, preferred_element_type=jnp.float32).astype(
        jnp.bfloat16
    )
    queries, key_rows, decay_rows, value_rows = lax.optimization_barrier(
        (queries, key_rows, decay_rows, value_rows)
    )
    forget_logit = (
        decay_rows.astype(jnp.float32)
        + lax.dynamic_slice_in_dim(decay_bias, head_start, key_dim, 0)[None, :]
    )
    forget = jnp.exp(jax.nn.log_sigmoid(forget_logit) / gate_tau)
    state_out = (
        forget[:, None, :] * state_in
        + value_rows.astype(jnp.float32)[:, :, None] * key_rows.astype(jnp.float32)[:, None, :]
    )
    readout = jnp.einsum(
        "svk,sk->sv", state_out, queries.astype(jnp.float32), precision=lax.Precision.HIGHEST
    ).astype(jnp.bfloat16)
    partial_value = jnp.dot(readout, proj_weight, preferred_element_type=jnp.float32)
    attention = summed_on_arrival(partial_value.astype(jnp.bfloat16), TP, 1).astype(jnp.bfloat16)
    attention = lax.optimization_barrier(attention)
    own_rows = lax.dynamic_slice_in_dim(row_values, tp_index * part_width, part_width, 1)
    middle = (own_rows + attention.astype(jnp.float32)).astype(jnp.bfloat16)
    middle = lax.optimization_barrier(middle)
    middle_own = middle.astype(jnp.float32)
    square_sum = one_axis_at_a_time(jnp.sum(middle_own * middle_own, axis=-1), TP)
    scaled_own = middle_own * lax.rsqrt(square_sum / model_width + epsilon)[:, None]
    expert_in = (scaled_own * ffn_gain.astype(jnp.float32)).astype(jnp.bfloat16)
    expert_all = EPG * route_group[:, None] + route_pick
    capacity = max(2, 2 * seq_count // ep_count)
    slot_rows = ep_count * capacity
    slot_range = jnp.arange(slot_rows, dtype=jnp.int32)
    gate_local = expert_gate[0]
    up_local = expert_up[0]
    down_local = expert_down[0]
    hidden = gate_local.shape[1]
    own_experts = lax.dynamic_slice_in_dim(expert_all, ep_index * seq_count, seq_count, 0)
    own_slots = pair_slots(own_experts.reshape(1, TOPK * seq_count), ep_count).reshape(
        seq_count, TOPK
    )
    target = own_experts * capacity + own_slots
    select_flat = (
        (target[:, :, None] == slot_range).astype(jnp.bfloat16).reshape(TOPK * seq_count, slot_rows)
    )
    doubled = jnp.repeat(expert_in, TOPK, axis=0)
    outgoing = lax.dot_general(
        select_flat, doubled, (((0,), (0,)), ((), ())), preferred_element_type=jnp.float32
    ).astype(jnp.bfloat16)
    outgoing = outgoing.reshape(ep_count, capacity, part_width)
    arrived = lax.all_to_all(outgoing, EP, split_axis=0, concat_axis=0, tiled=True)
    flat_rows = arrived.reshape(-1, part_width)
    hidden_pre = jnp.concatenate(
        [
            jnp.dot(flat_rows, gate_local, preferred_element_type=jnp.float32),
            jnp.dot(flat_rows, up_local, preferred_element_type=jnp.float32),
        ],
        axis=1,
    )
    share = summed_on_arrival(hidden_pre.astype(jnp.bfloat16), TP, 0)
    active_share = (jax.nn.silu(share[:, :hidden]) * share[:, hidden:]).astype(jnp.bfloat16)
    active = collect(active_share, TP, 0)
    served = (
        jnp.dot(active, down_local, preferred_element_type=jnp.float32)
        .astype(jnp.bfloat16)
        .reshape(arrived.shape)
    )
    returned = core_and_chips(served, ("ep_0", "ep_1"), (1, 0), 0, 0)
    picked = jnp.dot(
        select_flat, returned.reshape(slot_rows, part_width), preferred_element_type=jnp.float32
    ).reshape(seq_count, TOPK, part_width)
    own_weight = lax.dynamic_slice_in_dim(route_weight, ep_index * seq_count, seq_count, 0)
    mixture = own_weight[:, 0:1] * picked[:, 0] + own_weight[:, 1:2] * picked[:, 1]
    resid_out = (middle_own + mixture).astype(jnp.bfloat16)
    return (resid_out, state_out)


def solution(mesh):
    split = Mesh(mesh.devices.reshape(32, 2, 4, 4), ("ep_0", "ep_1", "tp_0", "tp_1"))
    placed = (
        P(EP, None),
        P(EP, TP, None),
        P(),
        P(),
        P(),
        P(),
        P(None, TP),
        P(),
        P(TP, None),
        P(TP),
        P(EP, TP, None),
        P(EP, TP, None),
        P(EP, None, TP),
        P(),
        P(),
        P(),
    )
    return jax.shard_map(
        on_device,
        mesh=split,
        in_specs=placed,
        out_specs=(P(EP, TP), P(EP, TP, None)),
        check_vma=False,
    )
```

profile of v0, /device:TPU:1, one launch (start us, length us, event | category | flops | bytes accessed | tf_op | source)
XLA Modules:
  0.0 151.8 jit_solution(7686870765759742231)
XLA Ops:
  0.7 0.8 convert_element_type.88
  1.5 1.0 multiply_reduce_fusion
  2.6 1.3 convolution_convert_fusion.4
  3.9 1.4 convolution_convert_fusion.5
  5.3 1.4 fusion.2
  7.0 0.8 dynamic_slice.25
  8.2 0.9 fusion.24
  10.0 7.6 %all-to-all-start = ((bf16[16,32,128]{2,1,0:T(8,128)(2,1)}), bf16[16,32,128]{2,1,0:T(8,128)(2,1)S(1)}, u32[]{:S(2)}, u32[]{:S(2)}) async-start(bf16[16,32,128]{2,1,0:T(8,128)(2,1)} %bitcast.61), calls=%async_computation | async-start | bytes 262144 | tf_op jit(solution)/shard_map/all_to_all | solution.py:28
  17.6 0.7 convert_element_type.87
  18.4 0.8 fusion.34
  19.9 0.8 multiply_add_fusion.1
  20.7 3.8 %all-to-all-done = bf16[16,32,128]{2,1,0:T(8,128)(2,1)S(1)} async-done(((bf16[16,32,128]{2,1,0:T(8,128)(2,1)}), bf16[16,32,128]{2,1,0:T(8,128)(2,1)S(1)}, u32[]{:S(2)}, u32[]{:S(2)}) %all-to-all-start) | async-done | bytes 131104 | tf_op jit(solution)/shard_map/all_to_all | solution.py:28
  24.5 0.7 add_convert_fusion
  25.3 6.9 %psum.14 = f32[32]{0:T(128)S(1)} all-reduce(f32[32]{0:T(128)S(1)} %fusion.14), channel_id=1, replica_groups=mesh['ep_0'=32,'ep_1'=2,'tp_0'=4,'tp_1'=4] {'tp_0'}, use_global_device_ids=true, to_apply=%region_5.6 | all-reduce | flops 32 | bytes 256 | tf_op jit(solution)/shard_map/psum | solution.py:33
  32.3 6.6 %psum.15 = f32[32]{0:T(128)S(1)} all-reduce(f32[32]{0:T(128)S(1)} %psum.14), channel_id=1, replica_groups=mesh['ep_0'=32,'ep_1'=2,'tp_0'=4,'tp_1'=4] {'tp_1'}, use_global_device_ids=true, to_apply=%region_6.7 | all-reduce | flops 32 | bytes 256 | tf_op jit(solution)/shard_map/psum | solution.py:33
  39.2 57.3 %all_to_all.30 = bf16[64,2,128]{2,1,0:T(2,128)(2,1)S(1)} all-to-all(bf16[64,2,128]{2,1,0:T(2,128)(2,1)S(1)} %bitcast.68), channel_id=1, replica_groups=mesh['ep_0'=32,'ep_1'=2,'tp_0'=4,'tp_1'=4] {'ep_0','ep_1'}, dimensions={0} | all-to-all | bytes 65536 | tf_op jit(solution)/shard_map/all_to_all | solution.py:168
  96.8 9.4 %all_to_all.31 = bf16[16,8,512]{2,1,0:T(8,128)(2,1)S(1)} all-to-all(bf16[16,8,512]{2,1,0:T(8,128)(2,1)S(1)} %pad_maximum_fusion), channel_id=1, replica_groups=mesh['ep_0'=32,'ep_1'=2,'tp_0'=4,'tp_1'=4] {'tp_0','tp_1'}, dimensions={0} | all-to-all | bytes 262144 | tf_op jit(solution)/shard_map/all_to_all | solution.py:28
  106.3 9.6 %all_to_all.32 = bf16[16,8,256]{2,1,0:T(8,128)(2,1)S(1)} all-to-all(bf16[16,8,256]{2,1,0:T(8,128)(2,1)S(1)} %broadcast_in_dim.5), channel_id=1, replica_groups=mesh['ep_0'=32,'ep_1'=2,'tp_0'=4,'tp_1'=4] {'tp_0','tp_1'}, dimensions={0} | all-to-all | bytes 131072 | tf_op jit(solution)/shard_map/all_to_all | solution.py:44
  115.9 1.0 convolution_convert_fusion.3
  116.9 7.3 %all_to_all.33 = bf16[32,2,1,2,128]{4,3,0,2,1:T(2,128)(2,1)S(1)} all-to-all(bf16[32,2,1,2,128]{4,3,0,2,1:T(2,128)(2,1)S(1)} %copy.36), channel_id=1, replica_groups=mesh['ep_0'=32,'ep_1'=2,'tp_0'=4,'tp_1'=4] {'ep_1'}, dimensions={1} | all-to-all | bytes 65536 | tf_op jit(solution)/shard_map/all_to_all | solution.py:57
  124.8 3.9 %all-to-all-start.5 = ((bf16[32,2,1,2,128]{4,3,1,2,0:T(2,128)(2,1)}), bf16[32,2,1,2,128]{4,3,1,2,0:T(2,128)(2,1)S(1)}, u32[]{:S(2)}, u32[]{:S(2)}) async-start(bf16[32,2,1,2,128]{4,3,1,2,0:T(2,128)(2,1)} %copy.37), calls=%async_computation.5 | async-start | bytes 65536 | tf_op jit(solution)/shard_map/all_to_all | solution.py:57
  128.7 0.8 constant_dynamic-slice_fusion.1
  129.5 21.4 %all-to-all-done.5 = bf16[32,2,1,2,128]{4,3,1,2,0:T(2,128)(2,1)S(1)} async-done(((bf16[32,2,1,2,128]{4,3,1,2,0:T(2,128)(2,1)}), bf16[32,2,1,2,128]{4,3,1,2,0:T(2,128)(2,1)S(1)}, u32[]{:S(2)}, u32[]{:S(2)}) %all-to-all-start.5) | async-done | bytes 32800 | tf_op jit(solution)/shard_map/all_to_all | solution.py:57
  151.1 0.7 fusion.17
  (53 shorter events, 4.1 us)
Async XLA Ops:
  0.6 2.0 %copy-start = (bf16[2048,512]{1,0:T(8,128)(2,1)S(1)}, bf16[2048,512]{1,0:T(8,128)(2,1)}, u32[]{:S(2)}) copy-start(bf16[2048,512]{1,0:T(8,128)(2,1)} %param.21) | copy-start | bytes 6291460
  0.6 6.0 %copy-start.2 = (bf16[32,2048]{1,0:T(8,128)(2,1)S(1)}, bf16[32,2048]{1,0:T(8,128)(2,1)}, u32[]{:S(2)}) copy-start(bf16[32,2048]{1,0:T(8,128)(2,1)} %param.16) | copy-start | bytes 393220
  0.7 6.0 %copy-start.8 = (bf16[2048,64]{0,1:T(8,128)(2,1)S(1)}, bf16[2048,64]{0,1:T(8,128)(2,1)}, u32[]{:S(2)}) copy-start(bf16[2048,64]{0,1:T(8,128)(2,1)} %param.22) | copy-start | bytes 786436
  2.6 5.2 %copy-start.3 = (f32[32,64,128]{2,1,0:T(8,128)S(1)}, f32[32,64,128]{2,1,0:T(8,128)}, u32[]{:S(2)}) copy-start(f32[32,64,128]{2,1,0:T(8,128)} %param.17) | copy-start | bytes 3145732
  5.2 3.9 %copy-start.4 = (bf16[64,2048]{1,0:T(8,128)(2,1)S(1)}, bf16[64,2048]{1,0:T(8,128)(2,1)}, u32[]{:S(2)}) copy-start(bf16[64,2048]{1,0:T(8,128)(2,1)} %param.24) | copy-start | bytes 786436
  7.8 10.5 %copy-start.9 = (bf16[128]{0:T(256)(128)(2,1)S(1)}, bf16[128]{0:T(256)(128)(2,1)}, u32[]{:S(2)}) copy-start(bf16[128]{0:T(256)(128)(2,1)} %param.25) | copy-start | bytes 772
  7.8 10.5 %copy-start.7 = (s32[2048]{0:T(1024)S(1)}, s32[2048]{0:T(1024)}, u32[]{:S(2)}) copy-start(s32[2048]{0:T(1024)} %param.29) | copy-start | bytes 24580
  7.8 88.7 %copy-start.5 = (bf16[1,128,256]{2,1,0:T(8,128)(2,1)S(1)}, bf16[1,128,256]{2,1,0:T(8,128)(2,1)}, u32[]{:S(2)}) copy-start(bf16[1,128,256]{2,1,0:T(8,128)(2,1)} %param.27) | copy-start | bytes 196612
  8.2 107.7 %copy-start.1 = (f32[32,64,128]{2,1,0:T(8,128)}, f32[32,64,128]{2,1,0:T(8,128)S(1)}, u32[]{:S(2)}) copy-start(f32[32,64,128]{2,1,0:T(8,128)S(1)} %multiply_add_fusion) | copy-start | bytes 3145732
  8.2 88.4 %copy-start.6 = (bf16[1,128,256]{2,1,0:T(8,128)(2,1)S(1)}, bf16[1,128,256]{2,1,0:T(8,128)(2,1)}, u32[]{:S(2)}) copy-start(bf16[1,128,256]{2,1,0:T(8,128)(2,1)} %param.26) | copy-start | bytes 196612
  10.0 14.4 %all-to-all-start = ((bf16[16,32,128]{2,1,0:T(8,128)(2,1)}), bf16[16,32,128]{2,1,0:T(8,128)(2,1)S(1)}, u32[]{:S(2)}, u32[]{:S(2)}) async-start(bf16[16,32,128]{2,1,0:T(8,128)(2,1)} %bitcast.61), calls=%async_computation | async-start | bytes 262144 | tf_op jit(solution)/shard_map/all_to_all | solution.py:28
  124.8 26.1 %all-to-all-start.5 = ((bf16[32,2,1,2,128]{4,3,1,2,0:T(2,128)(2,1)}), bf16[32,2,1,2,128]{4,3,1,2,0:T(2,128)(2,1)S(1)}, u32[]{:S(2)}, u32[]{:S(2)}) async-start(bf16[32,2,1,2,128]{4,3,1,2,0:T(2,128)(2,1)} %copy.37), calls=%async_computation.5 | async-start | bytes 65536 | tf_op jit(solution)/shard_map/all_to_all | solution.py:57
where the time goes:
time: 152 us
  blocking collectives  97.1 us (64%)
  waiting for transfers between devices  25.2 us (17%)
  starting transfers between devices  11.4 us (8%)
  matrix products  7.15 us (5%)
  other arithmetic  6.56 us (4%)
  local copies, waits for them, and re-layouts  3.4 us (2%)
    all_to_all x1, blocking collectives, on_device(): lax.all_to_all(outgoing, EP, split_axis=0, concat_axis=0, tiled=True)  57.3 us
    all_to_all x1, waiting for transfers between devices, moved_by_axis(): lax.all_to_all(pieces, axes[k], split_axis=k, concat_axis=k, tiled=True)  21.4 us
    psum x2, blocking collectives, one_axis_at_a_time(): return functools.reduce(lax.psum, axes, shard)  13.5 us
    all_to_all x1, blocking collectives, copy_for_each(): lax.all_to_all(jnp.broadcast_to(shard[None], (devices, *shard.shape)), ax...  9.61 us
    all_to_all x1, blocking collectives, summed_on_arrival(): lax.all_to_all(pieces, axis, split_axis=0, concat_axis=0, tiled=True)  9.43 us
    all_to_all x1, starting transfers between devices, summed_on_arrival(): lax.all_to_all(pieces, axis, split_axis=0, concat_axis=0, tiled=True)  7.58 us
    all_to_all x1, blocking collectives, moved_by_axis(): lax.all_to_all(pieces, axes[k], split_axis=k, concat_axis=k, tiled=True)  7.29 us
    all_to_all x1, starting transfers between devices, moved_by_axis(): lax.all_to_all(pieces, axes[k], split_axis=k, concat_axis=k, tiled=True)  3.85 us
  transfers between devices with their start and end apart: 2, of which 2 were waited for; matrix products, arithmetic and copies ran while one was open for 3% of the time, Pallas kernels for 0%

commit v1 on v0

v1 whole, which is shorter than its diff:
```python
import functools

import jax
import jax.numpy as jnp
from jax import lax
from jax.experimental import pallas as pl
from jax.experimental.pallas import tpu as pltpu
from jax.sharding import PartitionSpec as P

MESH = pl.DeviceIdType.MESH
F32 = jnp.float32
BF16 = jnp.bfloat16

epsilon = 1e-06
gate_tau = 16.0

SEQ = 32
WIDTH = 2048
DK = 128
DV = 256
VC = 64
PART = 128
FF = 256
CHIPS = 32
EXPERTS = 64
SIDE = 4
TPN = 16
NEAR = 4


def plane_offsets():
    steps = [(a, b) for a in range(SIDE) for b in range(SIDE) if a or b]
    return sorted(steps, key=lambda s: -(min(s[0], SIDE - s[0]) + min(s[1], SIDE - s[1])))


def line_offsets():
    return sorted(range(CHIPS), key=lambda s: -min(s, CHIPS - s))


def dot(a, b, dims=((1,), (0,))):
    return lax.dot_general(a, b, (dims, ((), ())), preferred_element_type=F32)


def layer_kernel(
    resid,
    state_in,
    mix_gain,
    query_w,
    key_w,
    decay_w,
    value_w,
    decay_bias,
    proj_w,
    ffn_gain,
    gate_w,
    up_w,
    down_w,
    group,
    pick,
    weight,
    resid_out,
    state_out,
    resid_v,
    mix_v,
    wq,
    wk,
    wd,
    wv,
    bias_v,
    wp,
    gain_v,
    wg,
    wu,
    wo,
    group_v,
    pick_v,
    weight_v,
    state_v,
    cols,
    part_s,
    part_r,
    rows_s,
    rows_r,
    hid_s,
    hid_r,
    act_s,
    act_r,
    back_s,
    back_r,
    out_v,
    load_sem,
    store_sem,
    send_sem,
    recv_sem,
    near_sem,
):
    ep = lax.axis_index("ep")
    tp = lax.axis_index("tp")
    z = ep // 2
    core = lax.rem(ep, 2)
    y = tp // SIDE
    x = lax.rem(tp, SIDE)
    head = tp // (DV // VC)
    block = ep // (PART // SEQ)
    head_cols = pl.ds(pl.multiple_of(head * DK, DK), DK)
    block_cols = pl.ds(pl.multiple_of(block * PART, PART), PART)

    pairs = [
        (resid, resid_v),
        (mix_gain, mix_v),
        (query_w.at[:, head_cols], wq),
        (key_w.at[:, head_cols], wk),
        (decay_w.at[:, head_cols], wd),
        (value_w, wv),
        (decay_bias, bias_v),
        (state_in, state_v),
        (proj_w, wp),
        (ffn_gain, gain_v),
        (group, group_v),
        (pick.at[:, block_cols], pick_v),
        (weight.at[:, block_cols], weight_v),
        (gate_w.at[0], wg),
        (up_w.at[0], wu),
        (down_w.at[0], wo),
    ]
    loads = [pltpu.make_async_copy(a, b, load_sem.at[i]) for i, (a, b) in enumerate(pairs)]

    for copy in loads:
        copy.start()

    def line_peer(step, other=0):
        return {"ep": lax.rem(z + step + CHIPS, CHIPS) * 2 + lax.rem(core + other, 2)}

    plane = [
        lax.rem(y + a, SIDE) * SIDE + lax.rem(x + b, SIDE) for a, b in plane_offsets()
    ]
    barrier = pltpu.get_barrier_semaphore()
    near = [{"tp": j} for j in plane] + [line_peer(0, 1)]
    for step in range(NEAR, 0, -1):
        for other in (0, 1):
            near += [line_peer(step, other), line_peer(-step, other)]
    for peer in near:
        pl.semaphore_signal(barrier, inc=1, device_id=peer, device_id_type=MESH)

    def ready(*which):
        for i in which:
            loads[i].wait()

    ready(0, 1)
    values = resid_v[...].astype(F32)
    inverse = lax.rsqrt(jnp.mean(values * values, axis=-1, keepdims=True) + epsilon)
    mix = mix_v[...].astype(F32)
    normed = jnp.concatenate(
        [
            (values[:, j * 128 : (j + 1) * 128] * inverse * mix[j : j + 1, :]).astype(BF16)
            for j in range(WIDTH // 128)
        ],
        axis=1,
    )

    pl.semaphore_wait(barrier, len(near))
    for step in (NEAR, -NEAR):
        pl.semaphore_signal(near_sem.at[0], inc=1, device_id=line_peer(step), device_id_type=MESH)

    ready(2, 3, 4, 5, 6)
    queries = (dot(normed, wq[...]) * DK ** (-0.5)).astype(BF16).astype(F32)
    keys = dot(normed, wk[...]).astype(BF16).astype(F32)
    decay = dot(normed, wd[...]).astype(BF16).astype(F32)
    value_t = dot(wv[...], normed, ((1,), (1,))).astype(BF16).astype(F32)
    logit = decay + bias_v[pl.ds(head, 1), :]
    log_gate = jnp.minimum(logit, 0.0) - jnp.log(1.0 + jnp.exp(-jnp.abs(logit)))
    forget = jnp.exp(log_gate / gate_tau)

    ready(7)
    lane = lax.broadcasted_iota(jnp.int32, (VC, SEQ), 1)
    readout_t = jnp.zeros((VC, SEQ), F32)
    for t in range(SEQ):
        new = (
            forget[t : t + 1, :] * state_v[t]
            + value_t[:, t : t + 1] * keys[t : t + 1, :]
        )
        state_v[t] = new
        total = jnp.sum(new * queries[t : t + 1, :], axis=1, keepdims=True)
        readout_t = jnp.where(lane == t, total, readout_t)
    store = pltpu.make_async_copy(state_v, state_out, store_sem.at[0])
    store.start()

    ready(8)
    partial = dot(readout_t.astype(BF16), wp[...], ((0,), (0,)))
    for j in range(TPN):
        part_s[j] = partial[:, j * PART : (j + 1) * PART].astype(BF16)

    pl.semaphore_wait(near_sem.at[0], 2)
    for step in (2 * NEAR, -2 * NEAR):
        pl.semaphore_signal(near_sem.at[1], inc=1, device_id=line_peer(step), device_id_type=MESH)

    def send(src, dst, phase, peer):
        pltpu.make_async_remote_copy(
            src_ref=src,
            dst_ref=dst,
            send_sem=send_sem.at[phase],
            recv_sem=recv_sem.at[phase],
            device_id=peer,
            device_id_type=MESH,
        ).start()

    def settle(ref, sem, phase):
        rest = ref.at[pl.ds(0, ref.shape[0] - 1)]
        pltpu.make_async_copy(rest, rest, sem.at[phase]).wait()

    for j in plane:
        send(part_s.at[j], part_r.at[tp], 0, {"tp": j})
    part_r[pl.ds(tp, 1)] = part_s[pl.ds(tp, 1)]

    ready(9, 10, 11, 12)
    base = group_v[pl.ds(block, 1), :] * 4
    first = (base + pick_v[0:1, :]).astype(F32)
    second = (base + pick_v[1:2, :]).astype(F32)
    sub = lax.broadcasted_iota(jnp.int32, (8, PART), 0)
    packed = jnp.where(
        sub == 0,
        first,
        jnp.where(sub == 1, second, jnp.where(sub == 2, weight_v[0:1, :], weight_v[1:2, :])),
    )
    cols[...] = packed.T
    own = cols[pl.ds(pl.multiple_of(lax.rem(ep, PART // SEQ) * SEQ, SEQ), SEQ), :]
    lanes = lax.broadcasted_iota(jnp.int32, (SEQ, 2 * EXPERTS), 1)
    expert_lane = (lanes // 2).astype(F32)
    slot_lane = lax.rem(lanes, 2).astype(F32)
    pick_a = (own[:, 0:1] == expert_lane).astype(F32)
    pick_b = (own[:, 1:2] == expert_lane).astype(F32)
    below = (
        lax.broadcasted_iota(jnp.int32, (SEQ, SEQ), 1)
        < lax.broadcasted_iota(jnp.int32, (SEQ, SEQ), 0)
    ).astype(F32)
    both = pick_a + pick_b
    earlier = dot(below.astype(BF16), both.astype(BF16))
    here = (earlier == slot_lane).astype(F32)
    select = (both * here).astype(BF16)
    mixing = (own[:, 2:3] * pick_a + own[:, 3:4] * pick_b) * here
    mixing_hi = mixing.astype(BF16)
    mixing_lo = (mixing - mixing_hi.astype(F32)).astype(BF16)
    select_t = select.astype(F32).T.astype(BF16)
    own_rows = resid_v[:, pl.ds(pl.multiple_of(tp * PART, PART), PART)].astype(F32)

    settle(part_r, recv_sem, 0)
    attention = jnp.sum(part_r[...].astype(F32), axis=0).astype(BF16)
    middle = (own_rows + attention.astype(F32)).astype(BF16)

    rows_s.reshape(2 * EXPERTS, PART)[...] = dot(select_t, middle).astype(BF16)
    pl.semaphore_wait(near_sem.at[1], 2)

    def to_line(src, dst, phase):
        for step in line_offsets():
            for other in (0, 1):
                if step == 0 and other == 0:
                    continue
                there = line_peer(step, other)
                send(src.at[there["ep"]], dst.at[ep], phase, there)
        dst[pl.ds(ep, 1)] = src[pl.ds(ep, 1)]

    to_line(rows_s, rows_r, 1)
    ready(13, 14, 15)
    gain = gain_v[...].astype(F32)
    settle(rows_r, recv_sem, 1)
    rows = rows_r.reshape(2 * EXPERTS, PART)[...].astype(F32)
    squares = jnp.sum(rows * rows, axis=1, keepdims=True)
    squares = jnp.broadcast_to(squares, (2 * EXPERTS, 128))
    squares_hi = squares.astype(BF16).astype(F32)
    squares_lo = squares - squares_hi
    scaled = (rows * gain).astype(BF16)
    gate_part = dot(scaled, wg[...])
    up_part = dot(scaled, wu[...])

    def owners(top, bottom):
        shape = (TPN, 8, top.shape[1])
        return jnp.concatenate([top.reshape(shape), bottom.reshape(shape)], axis=1).astype(BF16)

    hid_s[:, :, 0:FF] = owners(gate_part, up_part)
    hid_s[:, :, FF : FF + 128] = owners(squares_hi, squares_lo)
    for j in plane:
        send(hid_s.at[j], hid_r.at[tp], 2, {"tp": j})
    hid_r[pl.ds(tp, 1)] = hid_s[pl.ds(tp, 1)]
    settle(hid_r, recv_sem, 2)
    total = jnp.sum(hid_r[...].astype(F32), axis=0)
    square_sum = total[0:8, FF : FF + 128] + total[8:16, FF : FF + 128]
    scale = lax.rsqrt(square_sum / WIDTH + epsilon)
    scale = jnp.concatenate([scale, scale], axis=1)
    gate_pre = total[0:8, 0:FF] * scale
    up_pre = total[8:16, 0:FF] * scale
    active = gate_pre / (1.0 + jnp.exp(-gate_pre)) * up_pre
    act_s[...] = jnp.concatenate([active[:, 0:128], active[:, 128:256]], axis=0).astype(BF16)

    for j in plane:
        send(act_s, act_r.at[tp], 3, {"tp": j})
    act_r[pl.ds(tp, 1)] = act_s[...].reshape(1, 16, 128)
    settle(act_r, recv_sem, 3)
    acts = act_r[...].astype(F32)
    low = acts[:, 0:8, :].reshape(128, 128).astype(BF16)
    high = acts[:, 8:16, :].reshape(128, 128).astype(BF16)
    served = dot(low, wo[0:128, :]) + dot(high, wo[128:256, :])

    back_s.reshape(2 * EXPERTS, PART)[...] = served.astype(BF16)
    to_line(back_s, back_r, 4)
    settle(back_r, recv_sem, 4)
    back = back_r.reshape(2 * EXPERTS, PART)[...]
    mixture = dot(mixing_hi, back) + dot(mixing_lo, back)
    out_v[...] = (middle.astype(F32) + mixture).astype(BF16)
    last = pltpu.make_async_copy(out_v, resid_out, store_sem.at[1])
    last.start()

    settle(part_s, send_sem, 0)
    settle(rows_s, send_sem, 1)
    settle(hid_s, send_sem, 2)
    settle(act_r, send_sem, 3)
    settle(back_s, send_sem, 4)
    store.wait()
    last.wait()


def on_device(
    resid_in,
    state_in,
    mix_gain,
    query_weight,
    key_weight,
    decay_weight,
    value_weight,
    decay_bias,
    proj_weight,
    ffn_gain,
    expert_gate,
    expert_up,
    expert_down,
    route_group,
    route_pick,
    route_weight,
):
    args = (
        resid_in,
        state_in,
        mix_gain.reshape(WIDTH // 128, 128),
        query_weight,
        key_weight,
        decay_weight,
        value_weight.T,
        decay_bias.reshape(-1, DK),
        proj_weight,
        ffn_gain.reshape(1, PART),
        expert_gate,
        expert_up,
        expert_down,
        route_group.reshape(-1, 128),
        route_pick.T,
        route_weight.T,
    )
    vmem = pltpu.VMEM
    return pl.pallas_call(
        layer_kernel,
        out_shape=(
            jax.ShapeDtypeStruct((SEQ, PART), BF16),
            jax.ShapeDtypeStruct((SEQ, VC, DK), F32),
        ),
        in_specs=[pl.BlockSpec(memory_space=pl.ANY)] * len(args),
        out_specs=[pl.BlockSpec(memory_space=pl.ANY)] * 2,
        scratch_shapes=[
            vmem((SEQ, WIDTH), BF16),
            vmem((WIDTH // 128, 128), BF16),
            vmem((WIDTH, DK), BF16),
            vmem((WIDTH, DK), BF16),
            vmem((WIDTH, DK), BF16),
            vmem((VC, WIDTH), BF16),
            vmem((4, DK), F32),
            vmem((VC, WIDTH), BF16),
            vmem((1, PART), BF16),
            vmem((PART, FF), BF16),
            vmem((PART, FF), BF16),
            vmem((FF, PART), BF16),
            vmem((16, 128), jnp.int32),
            vmem((2, PART), jnp.int32),
            vmem((2, PART), F32),
            vmem((SEQ, VC, DK), F32),
            vmem((PART, 8), F32),
            vmem((TPN, SEQ, PART), BF16),
            vmem((TPN, SEQ, PART), BF16),
            vmem((EXPERTS, 2, PART), BF16),
            vmem((EXPERTS, 2, PART), BF16),
            vmem((TPN, 16, FF + 128), BF16),
            vmem((TPN, 16, FF + 128), BF16),
            vmem((16, 128), BF16),
            vmem((TPN, 16, 128), BF16),
            vmem((EXPERTS, 2, PART), BF16),
            vmem((EXPERTS, 2, PART), BF16),
            vmem((SEQ, PART), BF16),
            pltpu.SemaphoreType.DMA((16,)),
            pltpu.SemaphoreType.DMA((2,)),
            pltpu.SemaphoreType.DMA((5,)),
            pltpu.SemaphoreType.DMA((5,)),
            pltpu.SemaphoreType.REGULAR((2,)),
        ],
        compiler_params=pltpu.CompilerParams(collective_id=0, has_side_effects=True),
    )(*args)


def solution(mesh):
    return jax.shard_map(
        on_device,
        mesh=mesh,
        in_specs=(
            P("ep", None),
            P("ep", "tp", None),
            P(),
            P(),
            P(),
            P(),
            P(None, "tp"),
            P(),
            P("tp", None),
            P("tp"),
            P("ep", "tp", None),
            P("ep", "tp", None),
            P("ep", None, "tp"),
            P(),
            P(),
            P(),
        ),
        out_specs=(P("ep", "tp"), P("ep", "tp", None)),
        check_vma=False,
    )
```

time: 152 us -> 71.1 us (0.47)
  blocking collectives: 97.1 us -> 0 us
  Pallas kernels: 0 us -> 66.7 us
  waiting for transfers between devices: 25.2 us -> 0 us
  starting transfers between devices: 11.4 us -> 0 us
  matrix products: 7.15 us -> 0 us
  other arithmetic: 6.56 us -> 0 us
    all_to_all x4 -> x0, blocking collectives: 83.6 us -> none  [the longest x1 57.3 us: on_device(): lax.all_to_all(outgoing, EP, split_axis=0, concat_axis=0, tiled=True)]
    pallas_call x0 -> x1, Pallas kernels: none -> 66.7 us  [on_device(): pl.pallas_call(layer_kernel, out_shape=(jax.ShapeDtypeStruct((SEQ, PART),...]
    all_to_all x2 -> x0, waiting for transfers between devices: 25.2 us -> none  [the longest x1 21.4 us: moved_by_axis(): lax.all_to_all(pieces, axes[k], split_axis=k, concat_axis=k, tiled=True)]
    psum x2 -> x0, blocking collectives: 13.5 us -> none  [one_axis_at_a_time(): return functools.reduce(lax.psum, axes, shard)]
    all_to_all x2 -> x0, starting transfers between devices: 11.4 us -> none  [the longest x1 7.58 us: summed_on_arrival(): lax.all_to_all(pieces, axis, split_axis=0, concat_axis=0, tiled=True)]
    dot_general x11 -> x0, matrix products: 7.15 us -> none  [the longest x1 1.41 us: on_device(): jnp.dot(normed_in, query_head, preferred_element_type=jnp.float32)]
    unnamed x20 -> x2, local copies, waits for them, and re-layouts: 0.06 us -> 3.6 us
    convert_element_type x10 -> x0, other arithmetic: 3.14 us -> none  [the longest x1 0.84 us: on_device(): mix_gain.astype(jnp.float32)]
  transfers between devices with their start and end apart: 2 -> 0, of which waited for: 2 -> 0; matrix products, arithmetic and copies ran while one was open for 3% -> 0% of each run, Pallas kernels for 0% -> 0%
where the time goes in v1:
time: 71.1 us; the launch traced here: 70.9 us
  Pallas kernels  66.7 us (94%)
  local copies, waits for them, and re-layouts  3.6 us (5%)
    pallas_call x1, Pallas kernels, on_device(): pl.pallas_call(layer_kernel, out_shape=(jax.ShapeDtypeStruct((SEQ, PART),...  66.7 us
    unnamed x2, local copies, waits for them, and re-layouts  3.6 us

profile of v1, /device:TPU:1, one launch (start us, length us, event | category | flops | bytes accessed | tf_op | source)
XLA Modules:
  0.0 70.9 jit_solution(16848825702345368301)
XLA Ops:
  0.6 66.7 %shard_map.167 = (bf16[32,128]{1,0:T(8,128)(2,1)}, f32[32,64,128]{2,1,0:T(8,128)}) custom-call(bf16[32,2048]{1,0:T(8,128)(2,1)} %resid.1, f32[32,64,128]{2,1,0:T(8,128)} %state_in.1, bf16[16,128]{1,0:T(8,128)(2,1)} %bitcast.11, bf16[2048,512]{1,0:T(8,128)(2,1)} %query_w.1, bf16[2048,512]{1,0:T(8,128)(2,1)} %key_w.1, bf16[2048,512]{1,0:T(8,128)(2,1)} %decay_w.1, ...), custom_call_target="tpu_custom_call" | custom-call | tf_op jit(solution)/shard_map/pallas_call | solution.py:358
  67.3 1.3 %copy.20 = bf16[32,128]{1,0:T(8,128)(2,1)} copy(bf16[32,128]{1,0:T(8,128)(2,1)} %get-tuple-element.4) | data formatting | bytes 16384
  68.6 2.3 %copy.21 = f32[32,64,128]{2,1,0:T(8,128)} copy(f32[32,64,128]{2,1,0:T(8,128)} %get-tuple-element.5) | data formatting | bytes 2097152

commit v2 on v1

--- a/solution.py
+++ b/solution.py
@@ -25,7 +25,7 @@
 EXPERTS = 64
 SIDE = 4
 TPN = 16
-NEAR = 4
+NEAR = 8
 
 
 def plane_offsets():
@@ -58,7 +58,9 @@
     group,
     pick,
     weight,
-    resid_out,
+    middle_out,
+    mixing_out,
+    back_out,
     state_out,
     resid_v,
     mix_v,
@@ -87,9 +89,7 @@
     act_r,
     back_s,
     back_r,
-    out_v,
     load_sem,
-    store_sem,
     send_sem,
     recv_sem,
     near_sem,
@@ -114,7 +114,7 @@
         (value_w, wv),
         (decay_bias, bias_v),
         (state_in, state_v),
-        (proj_w, wp),
+        (proj_w, wp.at[pl.ds(0, VC)]),
         (ffn_gain, gain_v),
         (group, group_v),
         (pick.at[:, block_cols], pick_v),
@@ -122,11 +122,9 @@
         (gate_w.at[0], wg),
         (up_w.at[0], wu),
         (down_w.at[0], wo),
+        (proj_w, wp.at[pl.ds(VC, VC)]),
     ]
     loads = [pltpu.make_async_copy(a, b, load_sem.at[i]) for i, (a, b) in enumerate(pairs)]
-
-    for copy in loads:
-        copy.start()
 
     def line_peer(step, other=0):
         return {"ep": lax.rem(z + step + CHIPS, CHIPS) * 2 + lax.rem(core + other, 2)}
@@ -135,12 +133,15 @@
         lax.rem(y + a, SIDE) * SIDE + lax.rem(x + b, SIDE) for a, b in plane_offsets()
     ]
     barrier = pltpu.get_barrier_semaphore()
-    near = [{"tp": j} for j in plane] + [line_peer(0, 1)]
+    near = []
     for step in range(NEAR, 0, -1):
         for other in (0, 1):
             near += [line_peer(step, other), line_peer(-step, other)]
+    near += [{"tp": j} for j in plane] + [line_peer(0, 1)]
     for peer in near:
         pl.semaphore_signal(barrier, inc=1, device_id=peer, device_id_type=MESH)
+    for copy in loads:
+        copy.start()
 
     def ready(*which):
         for i in which:
@@ -158,10 +159,6 @@
         axis=1,
     )
 
-    pl.semaphore_wait(barrier, len(near))
-    for step in (NEAR, -NEAR):
-        pl.semaphore_signal(near_sem.at[0], inc=1, device_id=line_peer(step), device_id_type=MESH)
-
     ready(2, 3, 4, 5, 6)
     queries = (dot(normed, wq[...]) * DK ** (-0.5)).astype(BF16).astype(F32)
     keys = dot(normed, wk[...]).astype(BF16).astype(F32)
@@ -172,27 +169,33 @@
     forget = jnp.exp(log_gate / gate_tau)
 
     ready(7)
-    lane = lax.broadcasted_iota(jnp.int32, (VC, SEQ), 1)
-    readout_t = jnp.zeros((VC, SEQ), F32)
-    for t in range(SEQ):
-        new = (
-            forget[t : t + 1, :] * state_v[t]
-            + value_t[:, t : t + 1] * keys[t : t + 1, :]
-        )
-        state_v[t] = new
-        total = jnp.sum(new * queries[t : t + 1, :], axis=1, keepdims=True)
-        readout_t = jnp.where(lane == t, total, readout_t)
-    store = pltpu.make_async_copy(state_v, state_out, store_sem.at[0])
-    store.start()
-
-    ready(8)
-    partial = dot(readout_t.astype(BF16), wp[...], ((0,), (0,)))
+    queries = queries.astype(BF16)
+    row = lax.broadcasted_iota(jnp.int32, (SEQ, 2 * VC), 0)
+    right = lax.broadcasted_iota(jnp.int32, (SEQ, 2 * VC), 1) // VC
+    readout = jnp.zeros((SEQ, 2 * VC), F32)
+    for t in range(0, SEQ, 2):
+        two = []
+        for u in (t, t + 1):
+            new = (
+                forget[u : u + 1, :] * state_v[u]
+                + value_t[:, u : u + 1] * keys[u : u + 1, :]
+            )
+            state_out[u] = new
+            two.append(new)
+        new = jnp.concatenate(two, axis=0)
+        high = new.astype(BF16)
+        low = (new - high.astype(F32)).astype(BF16)
+        read = dot(queries, high, ((1,), (1,))) + dot(queries, low, ((1,), (1,)))
+        readout = jnp.where(row == t + right, read, readout)
+
+    ready(8, 16)
+    partial = dot(readout.astype(BF16), wp[...])
     for j in range(TPN):
         part_s[j] = partial[:, j * PART : (j + 1) * PART].astype(BF16)
 
-    pl.semaphore_wait(near_sem.at[0], 2)
-    for step in (2 * NEAR, -2 * NEAR):
-        pl.semaphore_signal(near_sem.at[1], inc=1, device_id=line_peer(step), device_id_type=MESH)
+    pl.semaphore_wait(barrier, len(near))
+    for step in (NEAR, -NEAR):
+        pl.semaphore_signal(near_sem.at[0], inc=1, device_id=line_peer(step), device_id_type=MESH)
 
     def send(src, dst, phase, peer):
         pltpu.make_async_remote_copy(
@@ -238,17 +241,17 @@
     here = (earlier == slot_lane).astype(F32)
     select = (both * here).astype(BF16)
     mixing = (own[:, 2:3] * pick_a + own[:, 3:4] * pick_b) * here
-    mixing_hi = mixing.astype(BF16)
-    mixing_lo = (mixing - mixing_hi.astype(F32)).astype(BF16)
+    mixing_out[...] = mixing
     select_t = select.astype(F32).T.astype(BF16)
     own_rows = resid_v[:, pl.ds(pl.multiple_of(tp * PART, PART), PART)].astype(F32)
 
     settle(part_r, recv_sem, 0)
     attention = jnp.sum(part_r[...].astype(F32), axis=0).astype(BF16)
     middle = (own_rows + attention.astype(F32)).astype(BF16)
+    middle_out[...] = middle
 
     rows_s.reshape(2 * EXPERTS, PART)[...] = dot(select_t, middle).astype(BF16)
-    pl.semaphore_wait(near_sem.at[1], 2)
+    pl.semaphore_wait(near_sem.at[0], 2)
 
     def to_line(src, dst, phase):
         for step in line_offsets():
@@ -303,17 +306,24 @@
     back_s.reshape(2 * EXPERTS, PART)[...] = served.astype(BF16)
     to_line(back_s, back_r, 4)
     settle(back_r, recv_sem, 4)
-    back = back_r.reshape(2 * EXPERTS, PART)[...]
-    mixture = dot(mixing_hi, back) + dot(mixing_lo, back)
-    out_v[...] = (middle.astype(F32) + mixture).astype(BF16)
-    last = pltpu.make_async_copy(out_v, resid_out, store_sem.at[1])
-    last.start()
+    back_out[...] = back_r.reshape(2 * EXPERTS, PART)[...]
 
     settle(part_s, send_sem, 0)
     settle(rows_s, send_sem, 1)
     settle(hid_s, send_sem, 2)
     settle(act_r, send_sem, 3)
     settle(back_s, send_sem, 4)
+
+
+def output_kernel(middle, mixing, back, state, resid_out, state_out, out_v, sem):
+    store = pltpu.make_async_copy(state, state_out, sem.at[0])
+    store.start()
+    mixing_hi = mixing[...].astype(BF16)
+    mixing_lo = (mixing[...] - mixing_hi.astype(F32)).astype(BF16)
+    mixture = dot(mixing_hi, back[...]) + dot(mixing_lo, back[...])
+    out_v[...] = (middle[...].astype(F32) + mixture).astype(BF16)
+    last = pltpu.make_async_copy(out_v, resid_out, sem.at[1])
+    last.start()
     store.wait()
     last.wait()
 
@@ -355,14 +365,16 @@
         route_weight.T,
     )
     vmem = pltpu.VMEM
-    return pl.pallas_call(
+    middle, mixing, back, state = pl.pallas_call(
         layer_kernel,
         out_shape=(
-            jax.ShapeDtypeStruct((SEQ, PART), BF16),
-            jax.ShapeDtypeStruct((SEQ, VC, DK), F32),
+            pltpu.VMEM((SEQ, PART), BF16),
+            pltpu.VMEM((SEQ, 2 * EXPERTS), F32),
+            pltpu.VMEM((2 * EXPERTS, PART), BF16),
+            pltpu.VMEM((SEQ, VC, DK), F32),
         ),
         in_specs=[pl.BlockSpec(memory_space=pl.ANY)] * len(args),
-        out_specs=[pl.BlockSpec(memory_space=pl.ANY)] * 2,
+        out_specs=[pl.BlockSpec(memory_space=pltpu.VMEM)] * 4,
         scratch_shapes=[
             vmem((SEQ, WIDTH), BF16),
             vmem((WIDTH // 128, 128), BF16),
@@ -371,7 +383,7 @@
             vmem((WIDTH, DK), BF16),
             vmem((VC, WIDTH), BF16),
             vmem((4, DK), F32),
-            vmem((VC, WIDTH), BF16),
+            vmem((2 * VC, WIDTH), BF16),
             vmem((1, PART), BF16),
             vmem((PART, FF), BF16),
             vmem((PART, FF), BF16),
@@ -391,15 +403,24 @@
             vmem((TPN, 16, 128), BF16),
             vmem((EXPERTS, 2, PART), BF16),
             vmem((EXPERTS, 2, PART), BF16),
-            vmem((SEQ, PART), BF16),
-            pltpu.SemaphoreType.DMA((16,)),
-            pltpu.SemaphoreType.DMA((2,)),
+            pltpu.SemaphoreType.DMA((17,)),
             pltpu.SemaphoreType.DMA((5,)),
             pltpu.SemaphoreType.DMA((5,)),
-            pltpu.SemaphoreType.REGULAR((2,)),
+            pltpu.SemaphoreType.REGULAR((1,)),
         ],
         compiler_params=pltpu.CompilerParams(collective_id=0, has_side_effects=True),
     )(*args)
+    return pl.pallas_call(
+        output_kernel,
+        out_shape=(
+            jax.ShapeDtypeStruct((SEQ, PART), BF16),
+            jax.ShapeDtypeStruct((SEQ, VC, DK), F32),
+        ),
+        in_specs=[pl.BlockSpec(memory_space=pltpu.VMEM)] * 4,
+        out_specs=[pl.BlockSpec(memory_space=pl.ANY)] * 2,
+        scratch_shapes=[vmem((SEQ, PART), BF16), pltpu.SemaphoreType.DMA((2,))],
+        compiler_params=pltpu.CompilerParams(vmem_limit_bytes=4 << 20),
+    )(*(pltpu.with_memory_space_constraint(a, pltpu.VMEM) for a in (middle, mixing, back, state)))
 
 
 def solution(mesh):

time: 71.1 us -> 67 us (0.942)
  local copies, waits for them, and re-layouts: 3.6 us -> 0 us
    unnamed x2 -> x0, local copies, waits for them, and re-layouts: 3.6 us -> none
    pallas_call x1 -> x2, Pallas kernels: 66.7 us -> 66.2 us  [the longest x1 65.2 us: on_device(): pl.pallas_call(layer_kernel, out_shape=(pltpu.VMEM((SEQ, PART), BF16), pl...]
where the time goes in v2:
time: 67 us; the launch traced here: 66.9 us
  Pallas kernels  66.2 us (99%)
    pallas_call x1, Pallas kernels, on_device(): pl.pallas_call(layer_kernel, out_shape=(pltpu.VMEM((SEQ, PART), BF16), pl...  65.2 us

profile of v2, /device:TPU:1, one launch (start us, length us, event | category | flops | bytes accessed | tf_op | source)
XLA Modules:
  0.0 66.9 jit_solution(558698341595959169)
XLA Ops:
  0.6 65.2 %shard_map.167 = (bf16[32,128]{1,0:T(8,128)(2,1)S(1)}, f32[32,128]{1,0:T(8,128)S(1)}, bf16[128,128]{1,0:T(8,128)(2,1)S(1)}, f32[32,64,128]{2,1,0:T(8,128)S(1)}) custom-call(bf16[32,2048]{1,0:T(8,128)(2,1)} %resid.1, f32[32,64,128]{2,1,0:T(8,128)} %state_in.1, bf16[16,128]{1,0:T(8,128)(2,1)} %bitcast.11, bf16[2048,512]{1,0:T(8,128)(2,1)} %query_w.1, ...), custom_call_target="tpu_custom_call" | custom-call | tf_op jit(solution)/shard_map/pallas_call | solution.py:368
  65.9 1.0 %shard_map.168 = (bf16[32,128]{1,0:T(8,128)(2,1)}, f32[32,64,128]{2,1,0:T(8,128)}) custom-call(bf16[32,128]{1,0:T(8,128)(2,1)S(1)} %get-tuple-element.6.middle, f32[32,128]{1,0:T(8,128)S(1)} %get-tuple-element.7.mixing, bf16[128,128]{1,0:T(8,128)(2,1)S(1)} %get-tuple-element.8.back, f32[32,64,128]{2,1,0:T(8,128)S(1)} %get-tuple-element.9.state), custom_call_target="tpu_custom_call" | custom-call | tf_op jit(solution)/shard_map/pallas_call | solution.py:413

commit v3 on v2

--- a/solution.py
+++ b/solution.py
@@ -85,8 +85,6 @@
     rows_r,
     hid_s,
     hid_r,
-    act_s,
-    act_r,
     back_s,
     back_r,
     load_sem,
@@ -121,7 +119,7 @@
         (weight.at[:, block_cols], weight_v),
         (gate_w.at[0], wg),
         (up_w.at[0], wu),
-        (down_w.at[0], wo),
+        (down_w.at[0], wo.at[tp]),
         (proj_w, wp.at[pl.ds(VC, VC)]),
     ]
     loads = [pltpu.make_async_copy(a, b, load_sem.at[i]) for i, (a, b) in enumerate(pairs)]
@@ -207,13 +205,17 @@
             device_id_type=MESH,
         ).start()
 
-    def settle(ref, sem, phase):
-        rest = ref.at[pl.ds(0, ref.shape[0] - 1)]
+    def settle(ref, sem, phase, count=None):
+        rest = ref.at[pl.ds(0, ref.shape[0] - 1 if count is None else count)]
         pltpu.make_async_copy(rest, rest, sem.at[phase]).wait()
 
     for j in plane:
         send(part_s.at[j], part_r.at[tp], 0, {"tp": j})
     part_r[pl.ds(tp, 1)] = part_s[pl.ds(tp, 1)]
+
+    ready(15)
+    for j in reversed(plane):
+        send(wo.at[tp], wo.at[tp], 3, {"tp": j})
 
     ready(9, 10, 11, 12)
     base = group_v[pl.ds(block, 1), :] * 4
@@ -263,7 +265,8 @@
         dst[pl.ds(ep, 1)] = src[pl.ds(ep, 1)]
 
     to_line(rows_s, rows_r, 1)
-    ready(13, 14, 15)
+
+    ready(13, 14)
     gain = gain_v[...].astype(F32)
     settle(rows_r, recv_sem, 1)
     rows = rows_r.reshape(2 * EXPERTS, PART)[...].astype(F32)
@@ -292,27 +295,40 @@
     gate_pre = total[0:8, 0:FF] * scale
     up_pre = total[8:16, 0:FF] * scale
     active = gate_pre / (1.0 + jnp.exp(-gate_pre)) * up_pre
-    act_s[...] = jnp.concatenate([active[:, 0:128], active[:, 128:256]], axis=0).astype(BF16)
+    active = active.astype(BF16)
+
+    settle(wo, recv_sem, 3)
+    for j in range(TPN):
+        served = dot(active, wo[j])
+        back_s[4 * j : 4 * j + 4] = served.astype(BF16).reshape(4, 2, PART)
+
+    def give_back(j, b):
+        there = {"ep": tp * 4 + b, "tp": j}
+        send(back_s.at[j * 4 + b], back_r.at[ep], 4, there)
 
     for j in plane:
-        send(act_s, act_r.at[tp], 3, {"tp": j})
-    act_r[pl.ds(tp, 1)] = act_s[...].reshape(1, 16, 128)
-    settle(act_r, recv_sem, 3)
-    acts = act_r[...].astype(F32)
-    low = acts[:, 0:8, :].reshape(128, 128).astype(BF16)
-    high = acts[:, 8:16, :].reshape(128, 128).astype(BF16)
-    served = dot(low, wo[0:128, :]) + dot(high, wo[128:256, :])
-
-    back_s.reshape(2 * EXPERTS, PART)[...] = served.astype(BF16)
-    to_line(back_s, back_r, 4)
-    settle(back_r, recv_sem, 4)
+        for b in range(4):
+            give_back(j, b)
+    for b in range(4):
+        pl.when(tp * 4 + b != ep)(functools.partial(give_back, tp, b))
+    own_block = ep // 4 == tp
+
+    @pl.when(own_block)
+    def _():
+        back_r[pl.ds(ep, 1)] = back_s[pl.ds(ep, 1)]
+
+    def both_ends(sem):
+        pl.when(own_block)(lambda: settle(back_r, sem, 4, EXPERTS - 1))
+        pl.when(jnp.logical_not(own_block))(lambda: settle(back_r, sem, 4, EXPERTS))
+
+    both_ends(recv_sem)
     back_out[...] = back_r.reshape(2 * EXPERTS, PART)[...]
 
     settle(part_s, send_sem, 0)
     settle(rows_s, send_sem, 1)
     settle(hid_s, send_sem, 2)
-    settle(act_r, send_sem, 3)
-    settle(back_s, send_sem, 4)
+    settle(wo, send_sem, 3)
+    both_ends(send_sem)
 
 
 def output_kernel(middle, mixing, back, state, resid_out, state_out, out_v, sem):
@@ -387,7 +403,7 @@
             vmem((1, PART), BF16),
             vmem((PART, FF), BF16),
             vmem((PART, FF), BF16),
-            vmem((FF, PART), BF16),
+            vmem((TPN, FF, PART), BF16),
             vmem((16, 128), jnp.int32),
             vmem((2, PART), jnp.int32),
             vmem((2, PART), F32),
@@ -399,8 +415,6 @@
             vmem((EXPERTS, 2, PART), BF16),
             vmem((TPN, 16, FF + 128), BF16),
             vmem((TPN, 16, FF + 128), BF16),
-            vmem((16, 128), BF16),
-            vmem((TPN, 16, 128), BF16),
             vmem((EXPERTS, 2, PART), BF16),
             vmem((EXPERTS, 2, PART), BF16),
             pltpu.SemaphoreType.DMA((17,)),

time: 67 us -> 63.3 us (0.945)
  Pallas kernels: 66.2 us -> 62.5 us
    pallas_call x1, Pallas kernels: 65.2 us -> 61.5 us  [on_device(): pl.pallas_call(layer_kernel, out_shape=(pltpu.VMEM((SEQ, PART), BF16), pl...]
where the time goes in v3:
time: 63.3 us; the launch traced here: 63.2 us
  Pallas kernels  62.5 us (99%)
  between operations  0.64 us (1%)
    pallas_call x1, Pallas kernels, on_device(): pl.pallas_call(layer_kernel, out_shape=(pltpu.VMEM((SEQ, PART), BF16), pl...  61.5 us

profile of v3, /device:TPU:1, one launch (start us, length us, event | category | flops | bytes accessed | tf_op | source)
XLA Modules:
  0.0 63.2 jit_solution(13482579972734629279)
XLA Ops:
  0.6 61.5 %shard_map.167 = (bf16[32,128]{1,0:T(8,128)(2,1)S(1)}, f32[32,128]{1,0:T(8,128)S(1)}, bf16[128,128]{1,0:T(8,128)(2,1)S(1)}, f32[32,64,128]{2,1,0:T(8,128)S(1)}) custom-call(bf16[32,2048]{1,0:T(8,128)(2,1)} %resid.1, f32[32,64,128]{2,1,0:T(8,128)} %state_in.1, bf16[16,128]{1,0:T(8,128)(2,1)} %bitcast.11, bf16[2048,512]{1,0:T(8,128)(2,1)} %query_w.1, ...), custom_call_target="tpu_custom_call" | custom-call | tf_op jit(solution)/shard_map/pallas_call | solution.py:384
  62.2 1.0 %shard_map.168 = (bf16[32,128]{1,0:T(8,128)(2,1)}, f32[32,64,128]{2,1,0:T(8,128)}) custom-call(bf16[32,128]{1,0:T(8,128)(2,1)S(1)} %get-tuple-element.6.middle, f32[32,128]{1,0:T(8,128)S(1)} %get-tuple-element.7.mixing, bf16[128,128]{1,0:T(8,128)(2,1)S(1)} %get-tuple-element.8.back, f32[32,64,128]{2,1,0:T(8,128)S(1)} %get-tuple-element.9.state), custom_call_target="tpu_custom_call" | custom-call | tf_op jit(solution)/shard_map/pallas_call | solution.py:427

commit v4 on v3

--- a/solution.py
+++ b/solution.py
@@ -85,6 +85,8 @@
     rows_r,
     hid_s,
     hid_r,
+    sq_s,
+    sq_r,
     back_s,
     back_r,
     load_sem,
@@ -271,9 +273,7 @@
     settle(rows_r, recv_sem, 1)
     rows = rows_r.reshape(2 * EXPERTS, PART)[...].astype(F32)
     squares = jnp.sum(rows * rows, axis=1, keepdims=True)
-    squares = jnp.broadcast_to(squares, (2 * EXPERTS, 128))
-    squares_hi = squares.astype(BF16).astype(F32)
-    squares_lo = squares - squares_hi
+    sq_s[...] = jnp.broadcast_to(squares, (2 * EXPERTS, 128)).T[0:1, :]
     scaled = (rows * gain).astype(BF16)
     gate_part = dot(scaled, wg[...])
     up_part = dot(scaled, wu[...])
@@ -282,16 +282,21 @@
         shape = (TPN, 8, top.shape[1])
         return jnp.concatenate([top.reshape(shape), bottom.reshape(shape)], axis=1).astype(BF16)
 
-    hid_s[:, :, 0:FF] = owners(gate_part, up_part)
-    hid_s[:, :, FF : FF + 128] = owners(squares_hi, squares_lo)
+    hid_s[...] = owners(gate_part, up_part)
     for j in plane:
+        send(sq_s, sq_r.at[tp], 5, {"tp": j})
         send(hid_s.at[j], hid_r.at[tp], 2, {"tp": j})
+    sq_r[pl.ds(tp, 1)] = sq_s[...].reshape(1, 1, 128)
     hid_r[pl.ds(tp, 1)] = hid_s[pl.ds(tp, 1)]
     settle(hid_r, recv_sem, 2)
     total = jnp.sum(hid_r[...].astype(F32), axis=0)
-    square_sum = total[0:8, FF : FF + 128] + total[8:16, FF : FF + 128]
+    settle(sq_r, recv_sem, 5)
+    square_row = jnp.sum(sq_r[...], axis=0)
+    own_lane = lax.broadcasted_iota(jnp.int32, (8, 128), 1) == (
+        tp * 8 + lax.broadcasted_iota(jnp.int32, (8, 128), 0)
+    )
+    square_sum = jnp.sum(jnp.where(own_lane, square_row, 0.0), axis=1, keepdims=True)
     scale = lax.rsqrt(square_sum / WIDTH + epsilon)
-    scale = jnp.concatenate([scale, scale], axis=1)
     gate_pre = total[0:8, 0:FF] * scale
     up_pre = total[8:16, 0:FF] * scale
     active = gate_pre / (1.0 + jnp.exp(-gate_pre)) * up_pre
@@ -327,6 +332,7 @@
     settle(part_s, send_sem, 0)
     settle(rows_s, send_sem, 1)
     settle(hid_s, send_sem, 2)
+    settle(sq_r, send_sem, 5)
     settle(wo, send_sem, 3)
     both_ends(send_sem)
 
@@ -413,13 +419,15 @@
             vmem((TPN, SEQ, PART), BF16),
             vmem((EXPERTS, 2, PART), BF16),
             vmem((EXPERTS, 2, PART), BF16),
-            vmem((TPN, 16, FF + 128), BF16),
-            vmem((TPN, 16, FF + 128), BF16),
+            vmem((TPN, 16, FF), BF16),
+            vmem((TPN, 16, FF), BF16),
+            vmem((1, 128), F32),
+            vmem((TPN, 1, 128), F32),
             vmem((EXPERTS, 2, PART), BF16),
             vmem((EXPERTS, 2, PART), BF16),
             pltpu.SemaphoreType.DMA((17,)),
-            pltpu.SemaphoreType.DMA((5,)),
-            pltpu.SemaphoreType.DMA((5,)),
+            pltpu.SemaphoreType.DMA((6,)),
+            pltpu.SemaphoreType.DMA((6,)),
             pltpu.SemaphoreType.REGULAR((1,)),
         ],
         compiler_params=pltpu.CompilerParams(collective_id=0, has_side_effects=True),

time: 63.3 us -> 63.1 us (level)
  no operation moved by 1% of the time
where the time goes in v4:
time: 63.1 us; the launch traced here: 63 us
  Pallas kernels  62.3 us (99%)
  between operations  0.64 us (1%)
    pallas_call x1, Pallas kernels, on_device(): pl.pallas_call(layer_kernel, out_shape=(pltpu.VMEM((SEQ, PART), BF16), pl...  61.3 us

profile of v4, /device:TPU:1, one launch (start us, length us, event | category | flops | bytes accessed | tf_op | source)
XLA Modules:
  0.0 63.0 jit_solution(1640537454258964485)
XLA Ops:
  0.6 61.3 %shard_map.167 = (bf16[32,128]{1,0:T(8,128)(2,1)S(1)}, f32[32,128]{1,0:T(8,128)S(1)}, bf16[128,128]{1,0:T(8,128)(2,1)S(1)}, f32[32,64,128]{2,1,0:T(8,128)S(1)}) custom-call(bf16[32,2048]{1,0:T(8,128)(2,1)} %resid.1, f32[32,64,128]{2,1,0:T(8,128)} %state_in.1, bf16[16,128]{1,0:T(8,128)(2,1)} %bitcast.11, bf16[2048,512]{1,0:T(8,128)(2,1)} %query_w.1, ...), custom_call_target="tpu_custom_call" | custom-call | tf_op jit(solution)/shard_map/pallas_call | solution.py:390
  62.0 1.0 %shard_map.168 = (bf16[32,128]{1,0:T(8,128)(2,1)}, f32[32,64,128]{2,1,0:T(8,128)}) custom-call(bf16[32,128]{1,0:T(8,128)(2,1)S(1)} %get-tuple-element.6.middle, f32[32,128]{1,0:T(8,128)S(1)} %get-tuple-element.7.mixing, bf16[128,128]{1,0:T(8,128)(2,1)S(1)} %get-tuple-element.8.back, f32[32,64,128]{2,1,0:T(8,128)S(1)} %get-tuple-element.9.state), custom_call_target="tpu_custom_call" | custom-call | tf_op jit(solution)/shard_map/pallas_call | solution.py:435
